TPU v7x, 32 devices: a whole 2x2x4 slice. The times are simulated.
32 devices in a mesh: rep: 2 (over x), fs: 8 (over z, y), tp: 2 (over core).
Axes of the slice: x: 2, y: 2, z: 4, core: 2. Of those that a mesh axis runs over, the one named last changes fastest.
Arguments:
- tokens: bfloat16 [4096, 2048], P(('rep', 'fs', 'tp')), may hold values from -6 to 6
- mix_gain: float32 [2048], replicated, may hold values from 0.1 to 1.9
- conv_in_weight: bfloat16 [2048, 1024], P('fs', 'tp'), may hold values from -0.125 to 0.125
- gate_outer_weight: bfloat16 [2048, 1024], P('fs', 'tp'), may hold values from -0.125 to 0.125
- gate_inner_weight: bfloat16 [2048, 1024], P('fs', 'tp'), may hold values from -0.125 to 0.125
- conv_taps: float32 [3, 1024], P(None, 'tp'), may hold values from -3.5 to 3.5
- out_weight: bfloat16 [1024, 2048], P('tp', 'fs'), may hold values from -0.1875 to 0.1875
- ff_gain: float32 [2048], replicated, may hold values from 0.1 to 1.9
- up_weight: bfloat16 [2048, 8192], P('fs', 'tp'), may hold values from -0.125 to 0.125
- down_weight: bfloat16 [8192, 2048], P('tp', 'fs'), may hold values from -0.0625 to 0.0625
Outputs:
- layer_out: bfloat16 [4096, 2048], P(('rep', 'fs', 'tp'))
All inputs are finite; a program needn't handle non-finite values.
Results may differ from a plain program's by a relative error of at most 0.023.
Values may be sent and summed in bfloat16 or wider, within the bound.
A program may use at most 128 MiB of HBM per device.

v0:
```python
import jax
import jax.numpy as jnp
from jax import lax
from jax.sharding import PartitionSpec as P

eps = 1e-06


def rms_scale(values, gain):
    widened = values.astype(jnp.float32)
    inverse = lax.rsqrt(jnp.mean(widened * widened, axis=-1, keepdims=True) + eps)
    return (widened * inverse * gain).astype(jnp.bfloat16)


def on_device(
    tokens,
    mix_gain,
    conv_in_weight,
    gate_outer_weight,
    gate_inner_weight,
    conv_taps,
    out_weight,
    ff_gain,
    up_weight,
    down_weight,
):
    normed = rms_scale(tokens, mix_gain)
    gathered = lax.all_gather(normed, "tp", axis=0, tiled=True)
    seq_rows = gathered.shape[0]
    segment = (
        lax.all_gather(conv_in_weight, "fs", axis=0, tiled=True),
        lax.all_gather(gate_outer_weight, "fs", axis=0, tiled=True),
        lax.all_gather(gate_inner_weight, "fs", axis=0, tiled=True),
    )
    conv_input, gate_outer, gate_inner = tuple(
        (jnp.dot(gathered, weight, preferred_element_type=jnp.float32) for weight in segment)
    )
    conv_input = conv_input.astype(jnp.bfloat16)
    gate_outer = gate_outer.astype(jnp.bfloat16)
    gate_inner = gate_inner.astype(jnp.bfloat16)
    gated = gate_inner.astype(jnp.float32) * conv_input.astype(jnp.float32)
    padded = jnp.pad(gated, ((2, 0), (0, 0)))
    convolved = (
        conv_taps[0] * padded[0:seq_rows]
        + conv_taps[1] * padded[1 : seq_rows + 1]
        + conv_taps[2] * padded[2 : seq_rows + 2]
    )
    mixed = (gate_outer.astype(jnp.float32) * convolved).astype(jnp.bfloat16)
    out_full = lax.all_gather(out_weight, "fs", axis=1, tiled=True)
    lefts = mixed
    mix_total = lax.psum_scatter(
        jnp.dot(lefts, out_full, preferred_element_type=jnp.float32).astype(jnp.bfloat16),
        "tp",
        scatter_dimension=0,
        tiled=True,
    ).astype(jnp.float32)
    resid = (tokens.astype(jnp.float32) + mix_total).astype(jnp.bfloat16)
    normed_ff = rms_scale(resid, ff_gain)
    ff_gathered = lax.all_gather(normed_ff, "tp", axis=0, tiled=True)
    up_full = lax.all_gather(up_weight, "fs", axis=0, tiled=True)
    preact = jnp.dot(ff_gathered, up_full, preferred_element_type=jnp.float32)
    hidden = jnp.square(jax.nn.relu(preact)).astype(jnp.bfloat16)
    down_full = lax.all_gather(down_weight, "fs", axis=1, tiled=True)
    lefts = hidden
    ff_total = lax.psum_scatter(
        jnp.dot(lefts, down_full, preferred_element_type=jnp.float32).astype(jnp.bfloat16),
        "tp",
        scatter_dimension=0,
        tiled=True,
    ).astype(jnp.float32)
    return (resid.astype(jnp.float32) + ff_total).astype(jnp.bfloat16)


def solution(mesh):
    in_specs = (
        P(("rep", "fs", "tp"), None),
        P(),
        P("fs", "tp"),
        P("fs", "tp"),
        P("fs", "tp"),
        P(None, "tp"),
        P("tp", "fs"),
        P(),
        P("fs", "tp"),
        P("tp", "fs"),
    )
    out_specs = P(("rep", "fs", "tp"), None)
    return jax.shard_map(
        on_device, mesh=mesh, in_specs=in_specs, out_specs=out_specs, check_vma=False
    )
```

profile of v0, /device:TPU:0, one launch (start us, length us, event | category | flops | bytes accessed | tf_op | source)
XLA Modules:
  0.0 740.0 jit_solution(13610082769893983982)
XLA Ops:
  6.5 1.2 fusion.8
  7.8 2.0 fusion.10
  9.9 0.7 all-gather.15.cloned.1.call-update
  10.6 0.7 all-gather.13.cloned.1.call-update
  12.0 0.5 all-gather.17.cloned.1.call-update
  12.6 9.2 %all-gather.9.cloned.1.call-done = bf16[256,2048]{1,0:T(8,128)(2,1)} async-done(((bf16[128,2048]{1,0:T(8,128)(2,1)}), bf16[256,2048]{1,0:T(8,128)(2,1)}) %all-gather.9.cloned.1.call-update) | async-done | bytes 1048592 | tf_op jit(solution)/shard_map/all_gather | solution.py:28
  21.7 52.4 %all-gather.15.cloned.1.call-done = bf16[2048,512]{1,0:T(8,128)(2,1)} async-done(((bf16[256,512]{1,0:T(8,128)(2,1)}), bf16[2048,512]{1,0:T(8,128)(2,1)}) %all-gather.15.cloned.1.call-update) | async-done | bytes 2097168 | tf_op jit(solution)/shard_map/all_gather | solution.py:31
  74.2 2.6 fusion.7
  76.8 47.2 %all-gather.13.cloned.1.call-done = bf16[2048,512]{1,0:T(8,128)(2,1)} async-done(((bf16[256,512]{1,0:T(8,128)(2,1)}), bf16[2048,512]{1,0:T(8,128)(2,1)}) %all-gather.13.cloned.1.call-update) | async-done | bytes 2097168 | tf_op jit(solution)/shard_map/all_gather | solution.py:33
  124.0 2.3 fusion.6
  126.3 47.3 %all-gather.11.cloned.1.call-done = bf16[2048,512]{1,0:T(8,128)(2,1)} async-done(((bf16[256,512]{1,0:T(8,128)(2,1)}), bf16[2048,512]{1,0:T(8,128)(2,1)}) %all-gather.11.cloned.1.call-update) | async-done | bytes 2097168 | tf_op jit(solution)/shard_map/all_gather | solution.py:32
  173.6 50.8 %all-gather.17.cloned.1.call-done = bf16[512,2048]{1,0:T(8,128)(2,1)} async-done(((bf16[512,256]{1,0:T(8,128)(2,1)}), bf16[512,2048]{1,0:T(8,128)(2,1)}) %all-gather.17.cloned.1.call-update) | async-done | bytes 2097168 | tf_op jit(solution)/shard_map/all_gather | solution.py:49
  224.4 4.7 convolution_convert_fusion.1
  229.2 6.7 reduce-scatter.3.cloned.1.call-done
  235.9 1.3 fusion.12
  237.2 2.0 fusion.14
  239.3 0.7 all-gather.21.cloned.1.call-update
  240.0 0.7 all-gather.23.cloned.1.call-update
  240.8 8.9 %all-gather.19.cloned.1.call-done = bf16[256,2048]{1,0:T(8,128)(2,1)} async-done(((bf16[128,2048]{1,0:T(8,128)(2,1)}), bf16[256,2048]{1,0:T(8,128)(2,1)}) %all-gather.19.cloned.1.call-update) | async-done | bytes 1048592 | tf_op jit(solution)/shard_map/all_gather | solution.py:59
  249.6 230.6 %all-gather.21.cloned.1.call-done = bf16[2048,4096]{1,0:T(8,128)(2,1)} async-done(((bf16[256,4096]{1,0:T(8,128)(2,1)}), bf16[2048,4096]{1,0:T(8,128)(2,1)}) %all-gather.21.cloned.1.call-update) | async-done | bytes 16777232 | tf_op jit(solution)/shard_map/all_gather | solution.py:60
  480.2 227.6 %all-gather.23.cloned.1.call-done = bf16[4096,2048]{1,0:T(8,128)(2,1)} async-done(((bf16[4096,256]{1,0:T(8,128)(2,1)}), bf16[4096,2048]{1,0:T(8,128)(2,1)}) %all-gather.23.cloned.1.call-update) | async-done | bytes 16777232 | tf_op jit(solution)/shard_map/all_gather | solution.py:63
  707.8 16.5 %convolution_convert_fusion = bf16[256,2048]{1,0:T(8,128)(2,1)} fusion(bf16[4096,2048]{1,0:T(8,128)(2,1)} %all-gather.23.cloned.1.call-done, bf16[256,2048]{1,0:T(8,128)(2,1)} %all-gather.19.cloned.1.call-done, bf16[2048,4096]{1,0:T(8,128)(2,1)} %all-gather.21.cloned.1.call-done), kind=kOutput, calls=%fused_computation.3 | convolution fusion | flops 8593604608 | bytes 35651584 | tf_op jit(solution)/shard_map/dot_general | solution.py:66
  724.4 6.7 reduce-scatter.5.cloned.1.call-done
  731.1 2.1 fusion.15
  (28 shorter events, 1.0 us)
Async XLA Ops:
  6.5 6.0 copy-start.4
  6.5 15.2 %all-gather.9.cloned.1.call-start = ((), (), s32[]{:S(2)}) async-start(), calls=%async_computation.2 | async-start | bytes 1572864 | tf_op jit(solution)/shard_map/all_gather | solution.py:28
  9.8 64.3 %all-gather.15.cloned.1.call-start = ((), (), s32[]{:S(2)}) async-start(), calls=%async_computation.5 | async-start | bytes 2359296 | tf_op jit(solution)/shard_map/all_gather | solution.py:31
  10.6 113.4 %all-gather.13.cloned.1.call-start = ((), (), s32[]{:S(2)}) async-start(), calls=%async_computation.4 | async-start | bytes 2359296 | tf_op jit(solution)/shard_map/all_gather | solution.py:33
  11.3 162.3 %all-gather.11.cloned.1.call-start = ((), (), s32[]{:S(2)}) async-start(), calls=%async_computation.3 | async-start | bytes 2359296 | tf_op jit(solution)/shard_map/all_gather | solution.py:32
  11.9 212.5 %all-gather.17.cloned.1.call-start = ((), (), s32[]{:S(2)}) async-start(), calls=%async_computation.6 | async-start | bytes 2359296 | tf_op jit(solution)/shard_map/all_gather | solution.py:49
  12.5 223.4 %reduce-scatter.3.cloned.1.call-start = ((), (), s32[]{:S(2)}) async-start(), calls=%async_computation.7 | async-start | bytes 1572864 | tf_op jit(solution)/shard_map/reduce_scatter | solution.py:51
  21.7 102.2 %copy-start.2 = (bf16[256,2048]{1,0:T(8,128)(2,1)S(1)}, bf16[256,2048]{1,0:T(8,128)(2,1)}, u32[]{:S(2)}) copy-start(bf16[256,2048]{1,0:T(8,128)(2,1)} %all-gather.9.cloned.1.call-done) | copy-start | bytes 3145732
  224.4 11.5 %copy-start = (bf16[128,2048]{1,0:T(8,128)(2,1)S(1)}, bf16[128,2048]{1,0:T(8,128)(2,1)}, u32[]{:S(2)}) copy-start(bf16[128,2048]{1,0:T(8,128)(2,1)} %param.10) | copy-start | bytes 1572868
  229.1 8.1 %copy-start.3 = (f32[2048]{0:T(1024)S(1)}, f32[2048]{0:T(1024)}, u32[]{:S(2)}) copy-start(f32[2048]{0:T(1024)} %param.17) | copy-start | bytes 24580
  229.1 20.5 %all-gather.19.cloned.1.call-start = ((), (), s32[]{:S(2)}) async-start(), calls=%async_computation.8 | async-start | bytes 1572864 | tf_op jit(solution)/shard_map/all_gather | solution.py:59
  239.2 241.0 %all-gather.21.cloned.1.call-start = ((), (), s32[]{:S(2)}) async-start(), calls=%async_computation.9 | async-start | bytes 18874368 | tf_op jit(solution)/shard_map/all_gather | solution.py:60
  240.0 467.8 %all-gather.23.cloned.1.call-start = ((), (), s32[]{:S(2)}) async-start(), calls=%async_computation.10 | async-start | bytes 18874368 | tf_op jit(solution)/shard_map/all_gather | solution.py:63
  240.7 490.4 %copy-start.1 = (bf16[128,2048]{1,0:T(8,128)(2,1)S(1)}, bf16[128,2048]{1,0:T(8,128)(2,1)}, u32[]{:S(2)}) copy-start(bf16[128,2048]{1,0:T(8,128)(2,1)} %reduce-scatter.3.cloned.1.call-done) | copy-start | bytes 1572868
  240.7 490.4 %reduce-scatter.5.cloned.1.call-start = ((), (), s32[]{:S(2)}) async-start(), calls=%async_computation.11 | async-start | bytes 1572864 | tf_op jit(solution)/shard_map/reduce_scatter | solution.py:65
Sparse Core Ops, SparseCore 0:
  10.0 11.7 all-gather.8
  23.9 50.2 all-gather.14
  76.3 47.6 all-gather.12
  125.9 47.6 all-gather.10
  175.5 48.8 all-gather.16
  229.2 6.5 reduce-scatter.2
  239.3 10.2 all-gather.18
  251.7 228.4 all-gather.20
  482.3 225.4 all-gather.22
  724.5 6.5 reduce-scatter.4
where the time goes:
time: 740 us
  waiting for transfers between devices  691 us (93%)
  matrix products  26.2 us (4%)
  between operations  13.6 us (2%)
  other arithmetic  8.69 us (1%)
    all_gather x1, waiting for transfers between devices, on_device(): up_full = lax.all_gather(up_weight, 'fs', axis=0, tiled=True)  231 us
    all_gather x1, waiting for transfers between devices, on_device(): down_full = lax.all_gather(down_weight, 'fs', axis=1, tiled=True)  228 us
    all_gather x1, waiting for transfers between devices, on_device(): lax.all_gather(conv_in_weight, 'fs', axis=0, tiled=True)  52.4 us
    all_gather x1, waiting for transfers between devices, on_device(): out_full = lax.all_gather(out_weight, 'fs', axis=1, tiled=True)  50.8 us
    all_gather x1, waiting for transfers between devices, on_device(): lax.all_gather(gate_outer_weight, 'fs', axis=0, tiled=True)  47.3 us
    all_gather x1, waiting for transfers between devices, on_device(): lax.all_gather(gate_inner_weight, 'fs', axis=0, tiled=True)  47.2 us
    dot_general x1, matrix products, on_device(): jnp.dot(lefts, down_full, preferred_element_type=jnp.float32)  16.5 us
  transfers between devices with their start and end apart: 10, of which 10 were waited for; matrix products, arithmetic and copies ran while one was open for 1% of the time, Pallas kernels for 0%

commit v1 on v0

--- a/solution.py
+++ b/solution.py
@@ -4,6 +4,16 @@
 from jax.sharding import PartitionSpec as P
 
 eps = 1e-06
+
+
+def gather_by_hops(x, axis, along):
+    peers = lax.axis_size(axis)
+    moving, blocks = (x, [x])
+    for _ in range(peers - 1):
+        moving = lax.ppermute(moving, axis, [(i, (i + 1) % peers) for i in range(peers)])
+        blocks.insert(0, moving)
+    row_of_blocks = jnp.concatenate(blocks, axis=along)
+    return jnp.roll(row_of_blocks, (lax.axis_index(axis) + 1) * x.shape[along], axis=along)
 
 
 def rms_scale(values, gain):
@@ -46,7 +56,7 @@
         + conv_taps[2] * padded[2 : seq_rows + 2]
     )
     mixed = (gate_outer.astype(jnp.float32) * convolved).astype(jnp.bfloat16)
-    out_full = lax.all_gather(out_weight, "fs", axis=1, tiled=True)
+    out_full = gather_by_hops(out_weight, "fs", 1)
     lefts = mixed
     mix_total = lax.psum_scatter(
         jnp.dot(lefts, out_full, preferred_element_type=jnp.float32).astype(jnp.bfloat16),

time: 740 us -> 704 us (0.951)
  waiting for transfers between devices: 691 us -> 639 us
  local copies, waits for them, and re-layouts: 0.03 us -> 12.8 us
    ppermute x0 -> x7, waiting for transfers between devices: none -> 84.9 us  [gather_by_hops(): lax.ppermute(moving, axis, [(i, (i + 1) % peers) for i in range(peers)])]
    all_gather x1, waiting for transfers between devices: 52.4 us -> 0.01 us  [on_device(): lax.all_gather(conv_in_weight, 'fs', axis=0, tiled=True)]
    all_gather x1 -> x0, waiting for transfers between devices: 50.8 us -> none  [on_device(): out_full = lax.all_gather(out_weight, 'fs', axis=1, tiled=True)]
    all_gather x1, waiting for transfers between devices: 47.2 us -> 23.5 us  [on_device(): lax.all_gather(gate_inner_weight, 'fs', axis=0, tiled=True)]
    unnamed x10 -> x25, local copies, waits for them, and re-layouts: 0.02 us -> 11.2 us
    all_gather x1, waiting for transfers between devices: 9.18 us -> 0.01 us  [on_device(): gathered = lax.all_gather(normed, 'tp', axis=0, tiled=True)]
  transfers between devices with their start and end apart: 10 -> 16, of which waited for: 10 -> 14; matrix products, arithmetic and copies ran while one was open for 1% -> 3% of each run, Pallas kernels for 0% -> 0%
where the time goes in v1:
time: 704 us
  waiting for transfers between devices  639 us (91%)
  matrix products  26.4 us (4%)
  between operations  13.3 us (2%)
  local copies, waits for them, and re-layouts  12.8 us (2%)
  other arithmetic  8.73 us (1%)
    all_gather x1, waiting for transfers between devices, on_device(): up_full = lax.all_gather(up_weight, 'fs', axis=0, tiled=True)  231 us
    all_gather x1, waiting for transfers between devices, on_device(): down_full = lax.all_gather(down_weight, 'fs', axis=1, tiled=True)  228 us
    ppermute x7, waiting for transfers between devices, gather_by_hops(): lax.ppermute(moving, axis, [(i, (i + 1) % peers) for i in range(peers)])  84.9 us
    all_gather x1, waiting for transfers between devices, on_device(): lax.all_gather(gate_outer_weight, 'fs', axis=0, tiled=True)  47 us
    all_gather x1, waiting for transfers between devices, on_device(): lax.all_gather(gate_inner_weight, 'fs', axis=0, tiled=True)  23.5 us
    dot_general x1, matrix products, on_device(): jnp.dot(lefts, down_full, preferred_element_type=jnp.float32)  16.5 us
  transfers between devices with their start and end apart: 16, of which 14 were waited for; matrix products, arithmetic and copies ran while one was open for 3% of the time, Pallas kernels for 0%

profile of v1, /device:TPU:0, one launch (start us, length us, event | category | flops | bytes accessed | tf_op | source)
XLA Modules:
  0.0 703.7 jit_solution(15362884891319000877)
XLA Ops:
  6.5 1.3 fusion.9
  7.8 2.0 fusion.11
  11.4 3.0 collective-permute-start
  14.5 9.6 %collective-permute-done = bf16[512,256]{1,0:T(8,128)(2,1)S(1)} collective-permute-done((bf16[512,256]{1,0:T(8,128)(2,1)}, bf16[512,256]{1,0:T(8,128)(2,1)S(1)}, u32[]{:S(2)}, u32[]{:S(2)}) %collective-permute-start) | collective-permute-done | bytes 262176 | tf_op jit(solution)/shard_map/ppermute | solution.py:13
  24.0 10.2 %collective-permute-done.1 = bf16[512,256]{1,0:T(8,128)(2,1)S(1)} collective-permute-done((bf16[512,256]{1,0:T(8,128)(2,1)S(1)}, bf16[512,256]{1,0:T(8,128)(2,1)S(1)}, u32[]{:S(2)}, u32[]{:S(2)}) %collective-permute-start.1) | collective-permute-done | bytes 262176 | tf_op jit(solution)/shard_map/ppermute | solution.py:13
  34.3 16.0 %collective-permute-done.2 = bf16[512,256]{1,0:T(8,128)(2,1)S(1)} collective-permute-done((bf16[512,256]{1,0:T(8,128)(2,1)S(1)}, bf16[512,256]{1,0:T(8,128)(2,1)S(1)}, u32[]{:S(2)}, u32[]{:S(2)}) %collective-permute-start.2) | collective-permute-done | bytes 262176 | tf_op jit(solution)/shard_map/ppermute | solution.py:13
  50.3 9.1 %collective-permute-done.3 = bf16[512,256]{1,0:T(8,128)(2,1)S(1)} collective-permute-done((bf16[512,256]{1,0:T(8,128)(2,1)S(1)}, bf16[512,256]{1,0:T(8,128)(2,1)S(1)}, u32[]{:S(2)}, u32[]{:S(2)}) %collective-permute-start.3) | collective-permute-done | bytes 262176 | tf_op jit(solution)/shard_map/ppermute | solution.py:13
  59.3 16.6 %collective-permute-done.4 = bf16[512,256]{1,0:T(8,128)(2,1)S(1)} collective-permute-done((bf16[512,256]{1,0:T(8,128)(2,1)S(1)}, bf16[512,256]{1,0:T(8,128)(2,1)S(1)}, u32[]{:S(2)}, u32[]{:S(2)}) %collective-permute-start.4) | collective-permute-done | bytes 262176 | tf_op jit(solution)/shard_map/ppermute | solution.py:13
  76.0 15.2 %collective-permute-done.5 = bf16[512,256]{1,0:T(8,128)(2,1)S(1)} collective-permute-done((bf16[512,256]{1,0:T(8,128)(2,1)S(1)}, bf16[512,256]{1,0:T(8,128)(2,1)S(1)}, u32[]{:S(2)}, u32[]{:S(2)}) %collective-permute-start.5) | collective-permute-done | bytes 262176 | tf_op jit(solution)/shard_map/ppermute | solution.py:13
  92.0 8.3 %collective-permute-done.6 = bf16[512,256]{1,0:T(8,128)(2,1)S(1)} collective-permute-done((bf16[512,256]{1,0:T(8,128)(2,1)S(1)}, bf16[512,256]{1,0:T(8,128)(2,1)S(1)}, u32[]{:S(2)}, u32[]{:S(2)}) %collective-permute-start.6) | collective-permute-done | bytes 262176 | tf_op jit(solution)/shard_map/ppermute | solution.py:13
  112.2 2.7 fusion.8
  114.9 23.5 %all-gather.12.cloned.1.call-done = bf16[2048,512]{1,0:T(8,128)(2,1)} async-done(((bf16[256,512]{1,0:T(8,128)(2,1)}), bf16[2048,512]{1,0:T(8,128)(2,1)}) %all-gather.12.cloned.1.call-update) | async-done | bytes 2097168 | tf_op jit(solution)/shard_map/all_gather | solution.py:43
  138.5 2.6 fusion.7
  141.1 47.0 %all-gather.10.cloned.1.call-done = bf16[2048,512]{1,0:T(8,128)(2,1)} async-done(((bf16[256,512]{1,0:T(8,128)(2,1)}), bf16[2048,512]{1,0:T(8,128)(2,1)}) %all-gather.10.cloned.1.call-update) | async-done | bytes 2097168 | tf_op jit(solution)/shard_map/all_gather | solution.py:42
  188.1 4.6 convolution_convert_fusion.1
  192.8 7.0 reduce-scatter.3.cloned.1.call-done
  199.8 1.3 fusion.13
  201.1 2.0 fusion.15
  204.8 8.9 %all-gather.16.cloned.1.call-done = bf16[256,2048]{1,0:T(8,128)(2,1)} async-done(((bf16[128,2048]{1,0:T(8,128)(2,1)}), bf16[256,2048]{1,0:T(8,128)(2,1)}) %all-gather.16.cloned.1.call-update) | async-done | bytes 1048592 | tf_op jit(solution)/shard_map/all_gather | solution.py:69
  213.6 230.6 %all-gather.18.cloned.1.call-done = bf16[2048,4096]{1,0:T(8,128)(2,1)} async-done(((bf16[256,4096]{1,0:T(8,128)(2,1)}), bf16[2048,4096]{1,0:T(8,128)(2,1)}) %all-gather.18.cloned.1.call-update) | async-done | bytes 16777232 | tf_op jit(solution)/shard_map/all_gather | solution.py:70
  444.2 227.6 %all-gather.20.cloned.1.call-done = bf16[4096,2048]{1,0:T(8,128)(2,1)} async-done(((bf16[4096,256]{1,0:T(8,128)(2,1)}), bf16[4096,2048]{1,0:T(8,128)(2,1)}) %all-gather.20.cloned.1.call-update) | async-done | bytes 16777232 | tf_op jit(solution)/shard_map/all_gather | solution.py:73
  671.8 16.5 %convolution_convert_fusion = bf16[256,2048]{1,0:T(8,128)(2,1)} fusion(bf16[4096,2048]{1,0:T(8,128)(2,1)} %all-gather.20.cloned.1.call-done, bf16[256,2048]{1,0:T(8,128)(2,1)} %all-gather.16.cloned.1.call-done, bf16[2048,4096]{1,0:T(8,128)(2,1)} %all-gather.18.cloned.1.call-done), kind=kOutput, calls=%fused_computation.3 | convolution fusion | flops 8593604608 | bytes 35651584 | tf_op jit(solution)/shard_map/dot_general | solution.py:76
  688.3 6.7 reduce-scatter.5.cloned.1.call-done
  695.0 2.1 fusion.16
  (55 shorter events, 16.0 us)
Async XLA Ops:
  6.5 99.0 %copy-start.2 = (bf16[512,256]{1,0:T(8,128)(2,1)S(1)}, bf16[512,256]{1,0:T(8,128)(2,1)}, u32[]{:S(2)}) copy-start(bf16[512,256]{1,0:T(8,128)(2,1)} %param.16) | copy-start | bytes 786436
  6.5 105.7 %all-gather.8.cloned.1.call-start = ((), (), s32[]{:S(2)}) async-start(), calls=%async_computation.2 | async-start | bytes 1572864 | tf_op jit(solution)/shard_map/all_gather | solution.py:38
  9.9 102.4 %all-gather.14.cloned.1.call-start = ((), (), s32[]{:S(2)}) async-start(), calls=%async_computation.5 | async-start | bytes 2359296 | tf_op jit(solution)/shard_map/all_gather | solution.py:41
  10.6 127.8 %all-gather.12.cloned.1.call-start = ((), (), s32[]{:S(2)}) async-start(), calls=%async_computation.4 | async-start | bytes 2359296 | tf_op jit(solution)/shard_map/all_gather | solution.py:43
  11.4 176.7 %all-gather.10.cloned.1.call-start = ((), (), s32[]{:S(2)}) async-start(), calls=%async_computation.3 | async-start | bytes 2359296 | tf_op jit(solution)/shard_map/all_gather | solution.py:42
  11.4 12.6 %collective-permute-start = (bf16[512,256]{1,0:T(8,128)(2,1)}, bf16[512,256]{1,0:T(8,128)(2,1)S(1)}, u32[]{:S(2)}, u32[]{:S(2)}) collective-permute-start(bf16[512,256]{1,0:T(8,128)(2,1)} %param.16), channel_id=1, source_target_pairs={{0,2},{2,4},{4,6},{6,8},{8,10},{10,12},{12,14},{14,0},{1,3},{3,5},... | collective-permute-start | bytes 786440 | tf_op jit(solution)/shard_map/ppermute | solution.py:13
  24.0 10.2 %collective-permute-start.1 = (bf16[512,256]{1,0:T(8,128)(2,1)S(1)}, bf16[512,256]{1,0:T(8,128)(2,1)S(1)}, u32[]{:S(2)}, u32[]{:S(2)}) collective-permute-start(bf16[512,256]{1,0:T(8,128)(2,1)S(1)} %collective-permute-done), channel_id=1, source_target_pairs={{0,2},{2,4},{4,6},{6,8},{8,10},{10,12},{12,14},{14,0},{1,3},{3,5},... | collective-permute-start | bytes 786440 | tf_op jit(solution)/shard_map/ppermute | solution.py:13
  34.2 16.1 %collective-permute-start.2 = (bf16[512,256]{1,0:T(8,128)(2,1)S(1)}, bf16[512,256]{1,0:T(8,128)(2,1)S(1)}, u32[]{:S(2)}, u32[]{:S(2)}) collective-permute-start(bf16[512,256]{1,0:T(8,128)(2,1)S(1)} %collective-permute-done.1), channel_id=1, source_target_pairs={{0,2},{2,4},{4,6},{6,8},{8,10},{10,12},{12,14},{14,0},{1,3},{3,5},... | collective-permute-start | bytes 786440 | tf_op jit(solution)/shard_map/ppermute | solution.py:13
  34.2 165.6 %reduce-scatter.3.cloned.1.call-start = ((), (), s32[]{:S(2)}) async-start(), calls=%async_computation.6 | async-start | bytes 1572864 | tf_op jit(solution)/shard_map/reduce_scatter | solution.py:61
  50.3 9.1 %collective-permute-start.3 = (bf16[512,256]{1,0:T(8,128)(2,1)S(1)}, bf16[512,256]{1,0:T(8,128)(2,1)S(1)}, u32[]{:S(2)}, u32[]{:S(2)}) collective-permute-start(bf16[512,256]{1,0:T(8,128)(2,1)S(1)} %collective-permute-done.2), channel_id=1, source_target_pairs={{0,2},{2,4},{4,6},{6,8},{8,10},{10,12},{12,14},{14,0},{1,3},{3,5},... | collective-permute-start | bytes 786440 | tf_op jit(solution)/shard_map/ppermute | solution.py:13
  59.3 16.6 %collective-permute-start.4 = (bf16[512,256]{1,0:T(8,128)(2,1)S(1)}, bf16[512,256]{1,0:T(8,128)(2,1)S(1)}, u32[]{:S(2)}, u32[]{:S(2)}) collective-permute-start(bf16[512,256]{1,0:T(8,128)(2,1)S(1)} %collective-permute-done.3), channel_id=1, source_target_pairs={{0,2},{2,4},{4,6},{6,8},{8,10},{10,12},{12,14},{14,0},{1,3},{3,5},... | collective-permute-start | bytes 786440 | tf_op jit(solution)/shard_map/ppermute | solution.py:13
  76.0 15.2 %collective-permute-start.5 = (bf16[512,256]{1,0:T(8,128)(2,1)S(1)}, bf16[512,256]{1,0:T(8,128)(2,1)S(1)}, u32[]{:S(2)}, u32[]{:S(2)}) collective-permute-start(bf16[512,256]{1,0:T(8,128)(2,1)S(1)} %collective-permute-done.4), channel_id=1, source_target_pairs={{0,2},{2,4},{4,6},{6,8},{8,10},{10,12},{12,14},{14,0},{1,3},{3,5},... | collective-permute-start | bytes 786440 | tf_op jit(solution)/shard_map/ppermute | solution.py:13
  91.1 9.1 %collective-permute-start.6 = (bf16[512,256]{1,0:T(8,128)(2,1)S(1)}, bf16[512,256]{1,0:T(8,128)(2,1)S(1)}, u32[]{:S(2)}, u32[]{:S(2)}) collective-permute-start(bf16[512,256]{1,0:T(8,128)(2,1)S(1)} %collective-permute-done.5), channel_id=1, source_target_pairs={{0,2},{2,4},{4,6},{6,8},{8,10},{10,12},{12,14},{14,0},{1,3},{3,5},... | collective-permute-start | bytes 786440 | tf_op jit(solution)/shard_map/ppermute | solution.py:13
  112.2 75.9 %copy-start.3 = (bf16[256,2048]{1,0:T(8,128)(2,1)S(1)}, bf16[256,2048]{1,0:T(8,128)(2,1)}, u32[]{:S(2)}) copy-start(bf16[256,2048]{1,0:T(8,128)(2,1)} %all-gather.8.cloned.1.call-done) | copy-start | bytes 3145732
  188.1 11.7 %copy-start = (bf16[128,2048]{1,0:T(8,128)(2,1)S(1)}, bf16[128,2048]{1,0:T(8,128)(2,1)}, u32[]{:S(2)}) copy-start(bf16[128,2048]{1,0:T(8,128)(2,1)} %param.10) | copy-start | bytes 1572868
  188.1 13.0 %copy-start.4 = (f32[2048]{0:T(1024)S(1)}, f32[2048]{0:T(1024)}, u32[]{:S(2)}) copy-start(f32[2048]{0:T(1024)} %param.17) | copy-start | bytes 24580
  192.8 20.9 %all-gather.16.cloned.1.call-start = ((), (), s32[]{:S(2)}) async-start(), calls=%async_computation.7 | async-start | bytes 1572864 | tf_op jit(solution)/shard_map/all_gather | solution.py:69
  203.2 241.0 %all-gather.18.cloned.1.call-start = ((), (), s32[]{:S(2)}) async-start(), calls=%async_computation.8 | async-start | bytes 18874368 | tf_op jit(solution)/shard_map/all_gather | solution.py:70
  204.0 467.8 %all-gather.20.cloned.1.call-start = ((), (), s32[]{:S(2)}) async-start(), calls=%async_computation.9 | async-start | bytes 18874368 | tf_op jit(solution)/shard_map/all_gather | solution.py:73
  204.7 490.3 %copy-start.1 = (bf16[128,2048]{1,0:T(8,128)(2,1)S(1)}, bf16[128,2048]{1,0:T(8,128)(2,1)}, u32[]{:S(2)}) copy-start(bf16[128,2048]{1,0:T(8,128)(2,1)} %reduce-scatter.3.cloned.1.call-done) | copy-start | bytes 1572868
  204.7 490.3 %reduce-scatter.5.cloned.1.call-start = ((), (), s32[]{:S(2)}) async-start(), calls=%async_computation.10 | async-start | bytes 1572864 | tf_op jit(solution)/shard_map/reduce_scatter | solution.py:75
Sparse Core Ops, SparseCore 0:
  10.0 11.7 all-gather.7
  23.9 61.6 all-gather.13
  87.8 50.6 all-gather.11
  140.4 47.6 all-gather.9
  192.9 6.8 reduce-scatter.2
  203.3 10.2 all-gather.15
  215.8 228.4 all-gather.17
  446.3 225.4 all-gather.19
  688.4 6.5 reduce-scatter.4
